TPU v7x, 32 devices: a whole 2x2x4 slice. The times are simulated.
32 devices in a mesh: ep: 16 (over z, x, core), tp: 2 (over y).
Axes of the slice: x: 2, y: 2, z: 4, core: 2. Of those that a mesh axis runs over, the one named last changes fastest.
Arguments:
- tokens: bfloat16 [256, 1024], P('ep'), may hold values from -6 to 6
- state: float32 [256, 16, 64, 64], P('ep', 'tp'), may hold values from -6 to 6
- w_recep: bfloat16 [1024, 1024], P(None, 'tp'), may hold values from -0.1875 to 0.1875
- w_key: bfloat16 [1024, 1024], P(None, 'tp'), may hold values from -0.1875 to 0.1875
- w_value: bfloat16 [1024, 1024], P(None, 'tp'), may hold values from -0.1875 to 0.1875
- w_out: bfloat16 [1024, 1024], P('tp'), may hold values from -0.1875 to 0.1875
- decay_base: float32 [1024], P('tp'), may hold values from -5 to 1
- decay_down: bfloat16 [1024, 64], replicated, may hold values from -0.1875 to 0.1875
- decay_up: bfloat16 [64, 1024], P(None, 'tp'), may hold values from -1 to 1
- rate_base: float32 [1024], P('tp'), may hold values from -4 to 4
- rate_down: bfloat16 [1024, 64], replicated, may hold values from -0.1875 to 0.1875
- rate_up: bfloat16 [64, 1024], P(None, 'tp'), may hold values from -1 to 1
- head_gain: float32 [1024], P('tp'), may hold values from 0.1 to 1.9
- first_gain: float32 [1024], replicated, may hold values from 0.2 to 4.8
- expert_gate: bfloat16 [16, 1024, 1408], P('ep', None, 'tp'), may hold values from -0.1875 to 0.1875
- expert_up: bfloat16 [16, 1024, 1408], P('ep', None, 'tp'), may hold values from -0.1875 to 0.1875
- expert_down: bfloat16 [16, 1408, 1024], P('ep', 'tp'), may hold values from -0.078125 to 0.078125
- dense_gate: bfloat16 [2816, 1024], P('ep'), may hold values from -0.1875 to 0.1875
- dense_up: bfloat16 [2816, 1024], P('ep'), may hold values from -0.1875 to 0.1875
- dense_down: bfloat16 [2816, 1024], P('ep', 'tp'), may hold values from -0.21875 to 0.21875
- branch_gate: bfloat16 [1024], replicated, may hold values from -0.1875 to 0.1875
- second_gain: float32 [1024], P('tp'), may hold values from 0.1 to 1.9
- routes: int32 [256, 2], P('ep'), may hold values from 0 to 3, all different within a row; in each aligned block of 16 rows (0 to 15, 16 to 31, ...) at most 16 rows name the same one
- route_weights: float32 [256, 2], P('ep'), may hold values from 0.2 to 1
Outputs:
- layer_output: bfloat16 [256, 1024], P('ep', 'tp')
Inputs may be any that keep to these rules, and one draw needn't show every extreme that they name: `routes`: each row names 2 different experts. In each aligned block of 16 rows no expert is named by more than 16 rows, a bound that some block reaches.
All inputs are finite; a program needn't handle non-finite values.
Results may differ from a plain program's by a relative error of at most 0.018.
Values may be sent and summed in bfloat16 or wider, within the bound.
A program may use at most 64 MiB of HBM per device.

v0:
```python
import jax
import jax.numpy as jnp
from jax import lax
from jax.sharding import PartitionSpec as P

SPLIT = 4
residual_scale = 1.4142135623730951
norm_epsilon = 1e-05
head_epsilon = 0.00064
key_epsilon = 1e-06


def time_mixer(
    tokens,
    state,
    w_recep,
    w_key,
    w_value,
    w_out,
    decay_base,
    decay_down,
    decay_up,
    rate_base,
    rate_down,
    rate_up,
    head_gain,
):
    row_count = tokens.shape[0]
    head_count = state.shape[1]
    head_size = state.shape[3]
    recep = jnp.dot(tokens, w_recep, preferred_element_type=jnp.float32).reshape(
        row_count, head_count, head_size
    )
    key_vecs = jnp.dot(tokens, w_key, preferred_element_type=jnp.float32).reshape(
        row_count, head_count, head_size
    )
    value_vecs = jnp.dot(tokens, w_value, preferred_element_type=jnp.float32).reshape(
        row_count, head_count, head_size
    )
    decay_low = jnp.tanh(jnp.dot(tokens, decay_down, preferred_element_type=jnp.float32)).astype(
        jnp.bfloat16
    )
    decay_pre = decay_base + jnp.dot(decay_low, decay_up, preferred_element_type=jnp.float32)
    log_rate = -jax.nn.softplus(-decay_pre) - 0.5
    decay = jnp.exp(-jnp.exp(log_rate)).reshape(row_count, head_count, head_size)
    rate_low = jnp.dot(tokens, rate_down, preferred_element_type=jnp.float32).astype(jnp.bfloat16)
    in_rate = jax.nn.sigmoid(
        rate_base + jnp.dot(rate_low, rate_up, preferred_element_type=jnp.float32)
    ).reshape(row_count, head_count, head_size)
    unit_keys = key_vecs * lax.rsqrt(jnp.sum(key_vecs * key_vecs, -1, keepdims=True) + key_epsilon)
    removed = jnp.einsum("bhij,bhj->bhi", state, -unit_keys)
    updated = (
        state * decay[:, :, None, :]
        + removed[..., None] * (unit_keys * in_rate)[:, :, None, :]
        + value_vecs[..., None] * key_vecs[:, :, None, :]
    )
    read_out = jnp.einsum("bhij,bhj->bhi", updated, recep)
    centre = jnp.mean(read_out, -1, keepdims=True)
    spread = jnp.mean(jnp.square(read_out - centre), -1, keepdims=True)
    normed = ((read_out - centre) * lax.rsqrt(spread + head_epsilon)).reshape(
        row_count, head_count * head_size
    ) * head_gain
    return jnp.dot(normed.astype(jnp.bfloat16), w_out, preferred_element_type=jnp.float32)


def first_norm(values, gain):
    centre = jnp.mean(values, -1, keepdims=True)
    spread = jnp.mean(jnp.square(values - centre), -1, keepdims=True)
    return ((values - centre) * lax.rsqrt(spread + norm_epsilon) * gain).astype(jnp.bfloat16)


def route_tables(routes, route_weights, experts, capacity):
    expert_hits = (
        routes[:, :, None] == jnp.arange(experts, dtype=jnp.int32)[None, None, :]
    ).astype(jnp.int32)
    row_hits = jnp.sum(expert_hits, 1, dtype=jnp.int32)
    earlier = jnp.cumsum(row_hits, 0, dtype=jnp.int32) - row_hits
    slot_index = jnp.sum(earlier[:, None, :] * expert_hits, 2, dtype=jnp.int32)
    target = routes * capacity + slot_index
    places = jnp.arange(experts * capacity, dtype=jnp.int32)
    slot_match = target[:, :, None] == places[None, None, :]
    dispatch_tokens = jnp.any(slot_match, 1).astype(jnp.bfloat16)
    combine_experts = jnp.sum(jnp.where(slot_match, route_weights[:, :, None], 0.0), 1)
    return (dispatch_tokens, combine_experts)


def shards(
    tokens,
    state,
    w_recep,
    w_key,
    w_value,
    w_out,
    decay_base,
    decay_down,
    decay_up,
    rate_base,
    rate_down,
    rate_up,
    head_gain,
    first_gain,
    expert_gate,
    expert_up,
    expert_down,
    dense_gate,
    dense_up,
    dense_down,
    branch_gate,
    second_gain,
    routes,
    route_weights,
):
    row_count = tokens.shape[0]
    model_width = tokens.shape[1]
    quarter = w_recep.shape[1]
    tp_index = lax.axis_index("tp")
    partial_mix = time_mixer(
        tokens,
        state,
        w_recep,
        w_key,
        w_value,
        w_out,
        decay_base,
        decay_down,
        decay_up,
        rate_base,
        rate_down,
        rate_up,
        head_gain,
    )
    mixed = lax.psum(partial_mix, "tp")
    x_mid = first_norm(residual_scale * tokens.astype(jnp.float32) + mixed, first_gain)
    own_columns = lax.dynamic_slice_in_dim(x_mid, tp_index * quarter, quarter, 1)
    experts = lax.axis_size("ep") // SPLIT
    capacity = min(row_count, max(2, 2 * row_count * routes.shape[1] // experts))
    dispatch_tokens, combine_experts = route_tables(routes, route_weights, experts, capacity)
    packed_rows = lax.dot_general(
        dispatch_tokens, x_mid, (((0,), (0,)), ((), ())), preferred_element_type=jnp.float32
    ).astype(jnp.bfloat16)
    outgoing = jnp.repeat(packed_rows.reshape(experts, capacity, x_mid.shape[1]), SPLIT, axis=0)
    arrived = lax.all_to_all(outgoing, "ep", split_axis=0, concat_axis=0, tiled=True)
    sources = arrived.shape[0]
    slot_count = arrived.shape[1]
    flat_rows = arrived.reshape(sources * slot_count, model_width)
    gate_pre = jnp.dot(flat_rows, expert_gate[0], preferred_element_type=jnp.float32)
    up_pre = jnp.dot(flat_rows, expert_up[0], preferred_element_type=jnp.float32)
    hidden = (jax.nn.silu(gate_pre) * up_pre).astype(jnp.bfloat16)
    partial_out = jnp.dot(hidden, expert_down[0], preferred_element_type=jnp.float32).reshape(
        sources, slot_count, model_width
    )
    summed = lax.psum_scatter(
        partial_out.astype(jnp.bfloat16), "tp", scatter_dimension=2, tiled=True
    ).astype(jnp.float32)
    returned = lax.all_to_all(
        summed.astype(jnp.bfloat16), "ep", split_axis=0, concat_axis=0, tiled=True
    ).astype(summed.dtype)
    expert_out = jnp.sum(returned.reshape(experts, SPLIT, capacity, quarter), 1).reshape(
        experts * capacity, quarter
    )
    routed_part = jnp.dot(
        combine_experts,
        expert_out,
        precision=lax.Precision.HIGHEST,
        preferred_element_type=jnp.float32,
    )
    branch = jax.nn.sigmoid(jnp.dot(x_mid, branch_gate, preferred_element_type=jnp.float32))
    shard_rows = lax.all_gather(x_mid, "ep", axis=0, tiled=True)
    gate_pre = lax.dot_general(
        shard_rows, dense_gate, (((1,), (1,)), ((), ())), preferred_element_type=jnp.float32
    )
    up_pre = lax.dot_general(
        shard_rows, dense_up, (((1,), (1,)), ((), ())), preferred_element_type=jnp.float32
    )
    dense_hidden = (jax.nn.silu(gate_pre) * up_pre).astype(jnp.bfloat16)
    dense_part = lax.psum_scatter(
        jnp.dot(dense_hidden, dense_down, preferred_element_type=jnp.float32),
        "ep",
        scatter_dimension=0,
        tiled=True,
    )
    second_sum = (
        residual_scale * own_columns.astype(jnp.float32)
        + routed_part
        + branch[:, None] * dense_part
    )
    row_sums, square_sums = lax.psum(
        (jnp.sum(second_sum, 1), jnp.sum(second_sum * second_sum, 1)), "tp"
    )
    average = row_sums / model_width
    spread = square_sums / model_width - average * average
    return (
        (second_sum - average[:, None]) * lax.rsqrt(spread + norm_epsilon)[:, None] * second_gain
    ).astype(jnp.bfloat16)


def solution(mesh):
    return jax.shard_map(
        shards,
        mesh=mesh,
        in_specs=(
            P("ep", None),
            P("ep", "tp", None, None),
            P(None, "tp"),
            P(None, "tp"),
            P(None, "tp"),
            P("tp", None),
            P("tp"),
            P(),
            P(None, "tp"),
            P("tp"),
            P(),
            P(None, "tp"),
            P("tp"),
            P(),
            P("ep", None, "tp"),
            P("ep", None, "tp"),
            P("ep", "tp", None),
            P("ep", None),
            P("ep", None),
            P("ep", "tp"),
            P(),
            P("tp"),
            P("ep", None),
            P("ep", None),
        ),
        out_specs=P("ep", "tp"),
        check_vma=False,
    )
```

profile of v0, /device:TPU:0, one launch (start us, length us, event | category | flops | bytes accessed | tf_op | source)
XLA Modules:
  0.0 162.2 jit_solution(11377209794120408051)
XLA Ops:
  6.5 0.0 copy-start
  6.5 0.0 all-reduce.3.cloned.1.call-start
  6.5 1.6 fusion.56
  8.1 0.1 reshape.96
  8.2 0.1 multiply_reduce_fusion.2
  8.3 1.2 fusion.32
  9.6 0.1 reshape.97
  9.6 1.5 fusion.59
  11.1 0.1 reshape.110
  11.2 1.3 fusion.49
  12.5 0.1 mul.167
  12.6 1.5 fusion.58
  14.0 0.1 mul.177
  14.1 0.1 multiply_negate_fusion
  14.2 3.5 %fusion.57 = f32[16,8,1,64]{3,2,1,0:T(1,128)S(1)} fusion(f32[16,8,64,1]{2,3,1,0:T(1,128)S(1)} %bitcast.81, f32[16,8,64,64]{3,2,1,0:T(8,128)} %param.25), kind=kOutput, calls=%fused_computation.85 | convolution fusion | flops 1048576 | bytes 2162688 | tf_op jit(solution)/shard_map/bhij,bhj->bhi/dot_general | solution.py:51
  17.8 0.0 copy-start.6
  17.8 0.0 copy-start.3
  17.8 2.9 %fusion = f32[16,8,1,64]{3,2,1,0:T(1,128)S(1)} fusion(f32[16,8,64,1]{2,3,1,0:T(1,128)S(1)} %bitcast.83, f32[16,8,64,64]{3,2,1,0:T(8,128)S(1)} %copy-done.1, f32[16,8,64]{2,1,0:T(8,128)S(1)} %reshape.96, f32[16,8,64]{2,1,0:T(8,128)S(1)} %mul.177, f32[16,8,64]{2,1,0:T(8,128)S(1)} %get-tuple-element.10, f32[16,8,64]{2,1,0:T(8,128)S(1)} %bitcast.82, ...), kind=kOutput, calls=%fused_computation | convolution fusion | flops 3670016 | bytes 2326528 | tf_op jit(solution)/shard_map/bhij,bhj->bhi/dot_general | solution.py:57
  20.7 0.1 reduce_sum.100
  20.8 0.2 multiply_reduce_fusion.1
  21.0 0.1 subtract_multiply_fusion
  21.1 0.1 reshape.99
  21.2 0.0 copy-done.7
  21.2 2.1 %fusion.51 = f32[16,1024]{1,0:T(8,128)} fusion(bf16[512,1024]{1,0:T(8,128)(2,1)} %param.29, f32[16,512]{1,0:T(8,128)S(1)} %reshape.99, f32[512]{0:T(512)S(1)} %copy-done.7), kind=kOutput, calls=%fused_computation.66 | convolution fusion | flops 16793600 | bytes 1148928 | tf_op jit(solution)/shard_map/dot_general | solution.py:63
  23.3 0.0 all-reduce.3.cloned.1.call-update
  23.3 0.0 reduce-scatter.3.cloned.1.call-start
  23.4 0.0 copy-done.5
  23.4 0.1 copy.33
  23.5 0.1 copy.35
  23.6 0.1 fusion.52
  23.7 23.4 %all-reduce.3.cloned.1.call-done = f32[16,1024]{1,0:T(8,128)} async-done(((f32[16,1024]{1,0:T(8,128)}), f32[16,1024]{1,0:T(8,128)}) %all-reduce.3.cloned.1.call-update) | async-done | bytes 65552 | tf_op jit(solution)/shard_map/psum | solution.py:132
  47.2 1.1 fusion.50
  48.2 1.0 multiply_reduce_fusion
  49.3 0.0 copy-done.6
  49.3 0.9 multiply_convert_fusion
  50.2 0.2 convolution_convert_fusion
  50.5 0.1 broadcast_in_dim.12
  50.5 19.7 %all_to_all.10 = bf16[16,16,1024]{2,1,0:T(8,128)(2,1)S(1)} all-to-all(bf16[16,16,1024]{2,1,0:T(8,128)(2,1)S(1)} %bitcast.72), channel_id=1, replica_groups=mesh['ep'=16,'tp'=2] {'ep'}, dimensions={0} | all-to-all | bytes 1048576 | tf_op jit(solution)/shard_map/all_to_all | solution.py:142
  70.2 0.6 fusion.15
  70.8 0.0 copy-start.4
  70.8 0.0 copy-start.12
  70.8 0.0 copy-start.13
  70.8 0.6 fusion.23
  71.4 0.0 copy-start.8
  71.4 0.0 copy-start.10
  71.4 0.2 copy.36
  71.6 0.0 copy-start.9
  71.6 0.0 copy-done
  71.6 1.4 fusion.17
  73.0 0.0 reduce-scatter.3.cloned.1.call-update
  73.1 0.0 reduce-scatter.5.cloned.1.call-start
  73.1 21.3 %all_gather.3 = bf16[256,1024]{1,0:T(8,128)(2,1)S(1)} all-gather(bf16[16,1024]{1,0:T(8,128)(2,1)S(1)} %multiply_convert_fusion), channel_id=1, replica_groups=mesh['ep'=16,'tp'=2] {'ep'}, dimensions={0}, use_global_device_ids=true | all-gather | bytes 557056 | tf_op jit(solution)/shard_map/all_gather | solution.py:168
  94.4 0.3 fusion.60
  94.8 1.5 fusion.27
  96.2 0.0 reduce-scatter.5.cloned.1.call-update
  96.3 0.0 reduce-scatter.3.cloned.1.call-done
  96.3 3.5 %all-to-all-start.1 = ((bf16[16,16,512]{2,1,0:T(8,128)(2,1)}), bf16[16,16,512]{2,1,0:T(8,128)(2,1)S(1)}, u32[]{:S(2)}, u32[]{:S(2)}) async-start(bf16[16,16,512]{2,1,0:T(8,128)(2,1)} %reduce-scatter.3.cloned.1.call-done), calls=%async_computation.2 | async-start | bytes 524288 | tf_op jit(solution)/shard_map/all_to_all | solution.py:155
  99.9 0.1 select_reduce_fusion
  100.0 0.1 fusion.38
  100.1 9.7 %all-to-all-done.1 = bf16[16,16,512]{2,1,0:T(8,128)(2,1)S(1)} async-done(((bf16[16,16,512]{2,1,0:T(8,128)(2,1)}), bf16[16,16,512]{2,1,0:T(8,128)(2,1)S(1)}, u32[]{:S(2)}, u32[]{:S(2)}) %all-to-all-start.1) | async-done | bytes 262176 | tf_op jit(solution)/shard_map/all_to_all | solution.py:155
  109.9 39.1 %reduce-scatter.5.cloned.1.call-done = f32[16,512]{1,0:T(8,128)} async-done(((f32[256,512]{1,0:T(8,128)}), f32[16,512]{1,0:T(8,128)}) %reduce-scatter.5.cloned.1.call-update) | async-done | bytes 32784 | tf_op jit(solution)/shard_map/reduce_scatter | solution.py:176
  148.9 1.1 fusion.55
  150.0 4.9 %all-reduce = (f32[16]{0:T(128)S(1)}, f32[16]{0:T(128)S(1)}) all-reduce(f32[16]{0:T(128)S(1)} %get-tuple-element.6, f32[16]{0:T(128)S(1)} %get-tuple-element.5), channel_id=1, replica_groups=mesh['ep'=16,'tp'=2] {'tp'}, use_global_device_ids=true, to_apply=%region_17.18 | all-reduce | flops 32 | bytes 256 | tf_op jit(solution)/shard_map/psum | solution.py:187
  154.9 0.7 multiply_convert_fusion.1
  (28 shorter events, 0.2 us)
Async XLA Ops:
  6.5 65.1 %copy-start = (bf16[1,704,1024]{2,1,0:T(8,128)(2,1)S(1)}, bf16[1,704,1024]{2,1,0:T(8,128)(2,1)}, u32[]{:S(2)}) copy-start(bf16[1,704,1024]{2,1,0:T(8,128)(2,1)} %param.40) | copy-start | bytes 4325380
  6.5 40.6 %all-reduce.3.cloned.1.call-start = ((), (), s32[]{:S(2)}) async-start(), calls=%async_computation.4 | async-start | bytes 131072 | tf_op jit(solution)/shard_map/psum | solution.py:132
  14.1 3.6 %copy-start.1 = (f32[16,8,64,64]{3,2,1,0:T(8,128)S(1)}, f32[16,8,64,64]{3,2,1,0:T(8,128)}, u32[]{:S(2)}) copy-start(f32[16,8,64,64]{3,2,1,0:T(8,128)} %param.25) | copy-start | bytes 6291460
  17.7 3.5 %copy-start.7 = (f32[512]{0:T(512)S(1)}, f32[512]{0:T(512)}, u32[]{:S(2)}) copy-start(f32[512]{0:T(512)} %param.36) | copy-start | bytes 6148
  17.7 5.6 %copy-start.5 = (s32[16,2]{0,1:T(2,128)S(1)}, s32[16,2]{0,1:T(2,128)}, u32[]{:S(2)}) copy-start(s32[16,2]{0,1:T(2,128)} %param.46) | copy-start | bytes 388
  17.7 29.4 %copy-start.2 = (bf16[16,1024]{1,0:T(8,128)(2,1)S(1)}, bf16[16,1024]{1,0:T(8,128)(2,1)}, u32[]{:S(2)}) copy-start(bf16[16,1024]{1,0:T(8,128)(2,1)} %param.24) | copy-start | bytes 98308
  17.8 31.5 %copy-start.6 = (f32[1024]{0:T(1024)S(1)}, f32[1024]{0:T(1024)}, u32[]{:S(2)}) copy-start(f32[1024]{0:T(1024)} %param.37) | copy-start | bytes 12292
  17.8 52.4 %copy-start.3 = (bf16[1,1024,704]{1,2,0:T(8,128)(2,1)S(1)}, bf16[1,1024,704]{1,2,0:T(8,128)(2,1)}, u32[]{:S(2)}) copy-start(bf16[1,1024,704]{1,2,0:T(8,128)(2,1)} %param.38) | copy-start | bytes 4325380
  23.3 73.0 %reduce-scatter.3.cloned.1.call-start = ((), (), s32[]{:S(2)}) async-start(), calls=%async_computation.5 | async-start | bytes 786432 | tf_op jit(solution)/shard_map/reduce_scatter | solution.py:152
  47.2 23.6 %copy-start.11 = (bf16[1,1024,704]{1,2,0:T(8,128)(2,1)S(1)}, bf16[1,1024,704]{1,2,0:T(8,128)(2,1)}, u32[]{:S(2)}) copy-start(bf16[1,1024,704]{1,2,0:T(8,128)(2,1)} %param.39) | copy-start | bytes 4325380
  70.8 23.6 %copy-start.4 = (bf16[176,1024]{1,0:T(8,128)(2,1)S(1)}, bf16[176,1024]{1,0:T(8,128)(2,1)}, u32[]{:S(2)}) copy-start(bf16[176,1024]{1,0:T(8,128)(2,1)} %param.41) | copy-start | bytes 1081348
  70.8 23.9 %copy-start.12 = (bf16[176,1024]{1,0:T(8,128)(2,1)S(1)}, bf16[176,1024]{1,0:T(8,128)(2,1)}, u32[]{:S(2)}) copy-start(bf16[176,1024]{1,0:T(8,128)(2,1)} %param.42) | copy-start | bytes 1081348
  70.8 23.9 %copy-start.13 = (bf16[176,512]{1,0:T(8,128)(2,1)S(1)}, bf16[176,512]{1,0:T(8,128)(2,1)}, u32[]{:S(2)}) copy-start(bf16[176,512]{1,0:T(8,128)(2,1)} %param.43) | copy-start | bytes 540676
  71.4 28.4 %copy-start.8 = (bf16[1024]{0:T(1024)(128)(2,1)S(1)}, bf16[1024]{0:T(1024)(128)(2,1)}, u32[]{:S(2)}) copy-start(bf16[1024]{0:T(1024)(128)(2,1)} %param.44) | copy-start | bytes 6148
  71.4 28.4 %copy-start.10 = (f32[16,2]{0,1:T(2,128)S(1)}, f32[16,2]{0,1:T(2,128)}, u32[]{:S(2)}) copy-start(f32[16,2]{0,1:T(2,128)} %param.47) | copy-start | bytes 388
  71.6 83.3 %copy-start.9 = (f32[512]{0:T(512)S(1)}, f32[512]{0:T(512)}, u32[]{:S(2)}) copy-start(f32[512]{0:T(512)} %param.45) | copy-start | bytes 6148
  73.1 75.9 %reduce-scatter.5.cloned.1.call-start = ((), (), s32[]{:S(2)}) async-start(), calls=%async_computation.6 | async-start | bytes 557056 | tf_op jit(solution)/shard_map/reduce_scatter | solution.py:176
  96.3 13.5 %all-to-all-start.1 = ((bf16[16,16,512]{2,1,0:T(8,128)(2,1)}), bf16[16,16,512]{2,1,0:T(8,128)(2,1)S(1)}, u32[]{:S(2)}, u32[]{:S(2)}) async-start(bf16[16,16,512]{2,1,0:T(8,128)(2,1)} %reduce-scatter.3.cloned.1.call-done), calls=%async_computation.2 | async-start | bytes 524288 | tf_op jit(solution)/shard_map/all_to_all | solution.py:155
Sparse Core Ops, SparseCore 0:
  23.4 23.6 all-reduce.2
  73.2 13.2 reduce-scatter.2
  96.4 52.5 reduce-scatter.4
where the time goes:
time: 163 us; the launch traced here: 162 us
  waiting for transfers between devices  72.3 us (44%)
  blocking collectives  45.9 us (28%)
  matrix products  21.3 us (13%)
  between operations  13.4 us (8%)
  other arithmetic  4.56 us (3%)
  starting transfers between devices  3.63 us (2%)
    reduce_scatter x1, waiting for transfers between devices, shards(): lax.psum_scatter(jnp.dot(dense_hidden, dense_down, preferred_element_type...  39.1 us
    psum x1, waiting for transfers between devices, shards(): mixed = lax.psum(partial_mix, 'tp')  23.4 us
    all_gather x1, blocking collectives, shards(): shard_rows = lax.all_gather(x_mid, 'ep', axis=0, tiled=True)  21.3 us
    all_to_all x1, blocking collectives, shards(): lax.all_to_all(outgoing, 'ep', split_axis=0, concat_axis=0, tiled=True)  19.7 us
    all_to_all x1, waiting for transfers between devices, shards(): lax.all_to_all(summed.astype(jnp.bfloat16), 'ep', split_axis=0, concat_ax...  9.73 us
    psum x1, blocking collectives, shards(): lax.psum((jnp.sum(second_sum, 1), jnp.sum(second_sum * second_sum, 1)), '...  4.93 us
    all_to_all x1, starting transfers between devices, shards(): lax.all_to_all(summed.astype(jnp.bfloat16), 'ep', split_axis=0, concat_ax...  3.54 us
    dot_general x1, matrix products, time_mixer(): removed = jnp.einsum('bhij,bhj->bhi', state, -unit_keys)  3.51 us
  transfers between devices with their start and end apart: 4, of which 3 were waited for; matrix products, arithmetic and copies ran while one was open for 1% of the time, Pallas kernels for 0%

commit v1 on v0

--- a/solution.py
+++ b/solution.py
@@ -165,7 +165,12 @@
         preferred_element_type=jnp.float32,
     )
     branch = jax.nn.sigmoid(jnp.dot(x_mid, branch_gate, preferred_element_type=jnp.float32))
-    shard_rows = lax.all_gather(x_mid, "ep", axis=0, tiled=True)
+    ring = [x_mid]
+    for hop in range(15):
+        ring.append(lax.ppermute(ring[-1], "ep", [(dev, (dev + 1) % 16) for dev in range(16)]))
+    shard_rows = jnp.roll(
+        jnp.concatenate(ring[::-1], axis=0), (lax.axis_index("ep") + 1) * ring[0].shape[0], axis=0
+    )
     gate_pre = lax.dot_general(
         shard_rows, dense_gate, (((1,), (1,)), ((), ())), preferred_element_type=jnp.float32
     )

time: 163 us -> 274 us (1.68)
  waiting for transfers between devices: 72.3 us -> 170 us
  local copies, waits for them, and re-layouts: 0.98 us -> 42.2 us
  blocking collectives: 45.9 us -> 4.93 us
  starting transfers between devices: 3.63 us -> 11.6 us
  matrix products: 21.3 us -> 24.8 us
    ppermute x0 -> x15, waiting for transfers between devices: none -> 84.2 us  [shards(): lax.ppermute(ring[-1], 'ep', [(dev, (dev + 1) % 16) for dev in range(16)])]
    unnamed x29 -> x80, local copies, waits for them, and re-layouts: 0.09 us -> 39.9 us
    all_gather x1 -> x0, blocking collectives: 21.3 us -> none  [shards(): shard_rows = lax.all_gather(x_mid, 'ep', axis=0, tiled=True)]
    all_to_all x1 -> x0, blocking collectives: 19.7 us -> none  [shards(): lax.all_to_all(outgoing, 'ep', split_axis=0, concat_axis=0, tiled=True)]
    reduce_scatter x1, waiting for transfers between devices: 0.02 us -> 8.14 us  [shards(): lax.psum_scatter(partial_out.astype(jnp.bfloat16), 'tp', scatter_dimensio...]
    all_to_all x0 -> x1, starting transfers between devices: none -> 5.83 us  [shards(): lax.all_to_all(outgoing, 'ep', split_axis=0, concat_axis=0, tiled=True)]
    reduce_scatter x1, waiting for transfers between devices: 39.1 us -> 44.1 us  [shards(): lax.psum_scatter(jnp.dot(dense_hidden, dense_down, preferred_element_type...]
  transfers between devices with their start and end apart: 4 -> 20, of which waited for: 3 -> 18; matrix products, arithmetic and copies ran while one was open for 1% -> 16% of each run, Pallas kernels for 0% -> 0%
where the time goes in v1:
time: 274 us; the launch traced here: 272 us
  waiting for transfers between devices  170 us (62%)
  local copies, waits for them, and re-layouts  42.2 us (15%)
  matrix products  24.8 us (9%)
  between operations  13.5 us (5%)
  starting transfers between devices  11.6 us (4%)
  blocking collectives  4.93 us (2%)
  other arithmetic  4.44 us (2%)
    ppermute x15, waiting for transfers between devices, shards(): lax.ppermute(ring[-1], 'ep', [(dev, (dev + 1) % 16) for dev in range(16)])  84.2 us
    reduce_scatter x1, waiting for transfers between devices, shards(): lax.psum_scatter(jnp.dot(dense_hidden, dense_down, preferred_element_type...  44.1 us
    unnamed x80, local copies, waits for them, and re-layouts  39.9 us
    psum x1, waiting for transfers between devices, shards(): mixed = lax.psum(partial_mix, 'tp')  23.8 us
    all_to_all x1, waiting for transfers between devices, shards(): lax.all_to_all(summed.astype(jnp.bfloat16), 'ep', split_axis=0, concat_ax...  9.77 us
    reduce_scatter x1, waiting for transfers between devices, shards(): lax.psum_scatter(partial_out.astype(jnp.bfloat16), 'tp', scatter_dimensio...  8.14 us
    all_to_all x1, starting transfers between devices, shards(): lax.all_to_all(outgoing, 'ep', split_axis=0, concat_axis=0, tiled=True)  5.83 us
    all_to_all x1, starting transfers between devices, shards(): lax.all_to_all(summed.astype(jnp.bfloat16), 'ep', split_axis=0, concat_ax...  5.62 us
  transfers between devices with their start and end apart: 20, of which 18 were waited for; matrix products, arithmetic and copies ran while one was open for 16% of the time, Pallas kernels for 0%

profile of v1, /device:TPU:0, one launch (start us, length us, event | category | flops | bytes accessed | tf_op | source)
XLA Modules:
  0.0 271.6 jit_solution(1051494662978393004)
XLA Ops:
  6.5 1.6 fusion.61
  8.3 1.2 fusion.30
  9.6 1.5 fusion.64
  11.2 1.3 fusion.51
  12.6 1.5 fusion.63
  14.2 3.5 %fusion.62 = f32[16,8,1,64]{3,2,1,0:T(1,128)S(1)} fusion(f32[16,8,64,1]{2,3,1,0:T(1,128)S(1)} %bitcast.78, f32[16,8,64,64]{3,2,1,0:T(8,128)} %param.25), kind=kOutput, calls=%fused_computation.117 | convolution fusion | flops 1048576 | bytes 2162688 | tf_op jit(solution)/shard_map/bhij,bhj->bhi/dot_general | solution.py:51
  17.8 2.9 %fusion = f32[16,8,1,64]{3,2,1,0:T(1,128)S(1)} fusion(f32[16,8,64,1]{2,3,1,0:T(1,128)S(1)} %bitcast.80, f32[16,8,64,64]{3,2,1,0:T(8,128)S(1)} %copy-done.1, f32[16,8,64]{2,1,0:T(8,128)S(1)} %reshape.96, f32[16,8,64]{2,1,0:T(8,128)S(1)} %mul.180, f32[16,8,64]{2,1,0:T(8,128)S(1)} %get-tuple-element.10, f32[16,8,64]{2,1,0:T(8,128)S(1)} %bitcast.79, ...), kind=kOutput, calls=%fused_computation | convolution fusion | flops 3670016 | bytes 2326528 | tf_op jit(solution)/shard_map/bhij,bhj->bhi/dot_general | solution.py:57
  21.2 2.1 fusion.53
  23.3 23.8 %all-reduce.3.cloned.1.call-done = f32[16,1024]{1,0:T(8,128)} async-done(((f32[16,1024]{1,0:T(8,128)}), f32[16,1024]{1,0:T(8,128)}) %all-reduce.3.cloned.1.call-update) | async-done | bytes 65552 | tf_op jit(solution)/shard_map/psum | solution.py:132
  47.2 1.0 fusion.52
  48.1 1.0 multiply_reduce_fusion
  49.2 0.9 multiply_convert_fusion.2
  50.2 6.0 %collective-permute-done = bf16[16,1024]{1,0:T(8,128)(2,1)S(1)} collective-permute-done((bf16[16,1024]{1,0:T(8,128)(2,1)S(1)}, bf16[16,1024]{1,0:T(8,128)(2,1)S(1)}, u32[]{:S(2)}, u32[]{:S(2)}) %collective-permute-start) | collective-permute-done | bytes 32800 | tf_op jit(solution)/shard_map/ppermute | solution.py:170
  56.2 6.0 %collective-permute-done.1 = bf16[16,1024]{1,0:T(8,128)(2,1)S(1)} collective-permute-done((bf16[16,1024]{1,0:T(8,128)(2,1)S(1)}, bf16[16,1024]{1,0:T(8,128)(2,1)S(1)}, u32[]{:S(2)}, u32[]{:S(2)}) %collective-permute-start.1) | collective-permute-done | bytes 32800 | tf_op jit(solution)/shard_map/ppermute | solution.py:170
  62.2 6.0 %collective-permute-done.2 = bf16[16,1024]{1,0:T(8,128)(2,1)S(1)} collective-permute-done((bf16[16,1024]{1,0:T(8,128)(2,1)S(1)}, bf16[16,1024]{1,0:T(8,128)(2,1)S(1)}, u32[]{:S(2)}, u32[]{:S(2)}) %collective-permute-start.2) | collective-permute-done | bytes 32800 | tf_op jit(solution)/shard_map/ppermute | solution.py:170
  68.3 6.0 %collective-permute-done.3 = bf16[16,1024]{1,0:T(8,128)(2,1)S(1)} collective-permute-done((bf16[16,1024]{1,0:T(8,128)(2,1)S(1)}, bf16[16,1024]{1,0:T(8,128)(2,1)S(1)}, u32[]{:S(2)}, u32[]{:S(2)}) %collective-permute-start.3) | collective-permute-done | bytes 32800 | tf_op jit(solution)/shard_map/ppermute | solution.py:170
  74.9 6.0 %collective-permute-done.4 = bf16[16,1024]{1,0:T(8,128)(2,1)S(1)} collective-permute-done((bf16[16,1024]{1,0:T(8,128)(2,1)S(1)}, bf16[16,1024]{1,0:T(8,128)(2,1)S(1)}, u32[]{:S(2)}, u32[]{:S(2)}) %collective-permute-start.4) | collective-permute-done | bytes 32800 | tf_op jit(solution)/shard_map/ppermute | solution.py:170
  81.6 6.0 %collective-permute-done.5 = bf16[16,1024]{1,0:T(8,128)(2,1)S(1)} collective-permute-done((bf16[16,1024]{1,0:T(8,128)(2,1)S(1)}, bf16[16,1024]{1,0:T(8,128)(2,1)S(1)}, u32[]{:S(2)}, u32[]{:S(2)}) %collective-permute-start.5) | collective-permute-done | bytes 32800 | tf_op jit(solution)/shard_map/ppermute | solution.py:170
  88.2 6.0 %collective-permute-done.6 = bf16[16,1024]{1,0:T(8,128)(2,1)S(1)} collective-permute-done((bf16[16,1024]{1,0:T(8,128)(2,1)S(1)}, bf16[16,1024]{1,0:T(8,128)(2,1)S(1)}, u32[]{:S(2)}, u32[]{:S(2)}) %collective-permute-start.6) | collective-permute-done | bytes 32800 | tf_op jit(solution)/shard_map/ppermute | solution.py:170
  94.8 6.0 %collective-permute-done.7 = bf16[16,1024]{1,0:T(8,128)(2,1)S(1)} collective-permute-done((bf16[16,1024]{1,0:T(8,128)(2,1)S(1)}, bf16[16,1024]{1,0:T(8,128)(2,1)S(1)}, u32[]{:S(2)}, u32[]{:S(2)}) %collective-permute-start.7) | collective-permute-done | bytes 32800 | tf_op jit(solution)/shard_map/ppermute | solution.py:170
  101.5 6.0 %collective-permute-done.8 = bf16[16,1024]{1,0:T(8,128)(2,1)S(1)} collective-permute-done((bf16[16,1024]{1,0:T(8,128)(2,1)S(1)}, bf16[16,1024]{1,0:T(8,128)(2,1)S(1)}, u32[]{:S(2)}, u32[]{:S(2)}) %collective-permute-start.8) | collective-permute-done | bytes 32800 | tf_op jit(solution)/shard_map/ppermute | solution.py:170
  108.1 6.0 %collective-permute-done.9 = bf16[16,1024]{1,0:T(8,128)(2,1)S(1)} collective-permute-done((bf16[16,1024]{1,0:T(8,128)(2,1)S(1)}, bf16[16,1024]{1,0:T(8,128)(2,1)S(1)}, u32[]{:S(2)}, u32[]{:S(2)}) %collective-permute-start.9) | collective-permute-done | bytes 32800 | tf_op jit(solution)/shard_map/ppermute | solution.py:170
  114.4 5.8 %collective-permute-done.10 = bf16[16,1024]{1,0:T(8,128)(2,1)S(1)} collective-permute-done((bf16[16,1024]{1,0:T(8,128)(2,1)S(1)}, bf16[16,1024]{1,0:T(8,128)(2,1)S(1)}, u32[]{:S(2)}, u32[]{:S(2)}) %collective-permute-start.10) | collective-permute-done | bytes 32800 | tf_op jit(solution)/shard_map/ppermute | solution.py:170
  120.2 6.0 %collective-permute-done.11 = bf16[16,1024]{1,0:T(8,128)(2,1)S(1)} collective-permute-done((bf16[16,1024]{1,0:T(8,128)(2,1)S(1)}, bf16[16,1024]{1,0:T(8,128)(2,1)S(1)}, u32[]{:S(2)}, u32[]{:S(2)}) %collective-permute-start.11) | collective-permute-done | bytes 32800 | tf_op jit(solution)/shard_map/ppermute | solution.py:170
  126.2 6.0 %collective-permute-done.12 = bf16[16,1024]{1,0:T(8,128)(2,1)S(1)} collective-permute-done((bf16[16,1024]{1,0:T(8,128)(2,1)S(1)}, bf16[16,1024]{1,0:T(8,128)(2,1)S(1)}, u32[]{:S(2)}, u32[]{:S(2)}) %collective-permute-start.12) | collective-permute-done | bytes 32800 | tf_op jit(solution)/shard_map/ppermute | solution.py:170
  132.3 6.1 %collective-permute-done.13 = bf16[16,1024]{1,0:T(8,128)(2,1)} collective-permute-done((bf16[16,1024]{1,0:T(8,128)(2,1)S(1)}, bf16[16,1024]{1,0:T(8,128)(2,1)}, u32[]{:S(2)}, u32[]{:S(2)}) %collective-permute-start.13) | collective-permute-done | bytes 32800 | tf_op jit(solution)/shard_map/ppermute | solution.py:170
  138.6 0.9 broadcast_in_dim.12
  139.5 5.8 %all-to-all-start = ((bf16[16,16,1024]{2,1,0:T(8,128)(2,1)}), bf16[16,16,1024]{2,1,0:T(8,128)(2,1)S(1)}, u32[]{:S(2)}, u32[]{:S(2)}) async-start(bf16[16,16,1024]{2,1,0:T(8,128)(2,1)} %bitcast.8), calls=%async_computation | async-start | bytes 1048576 | tf_op jit(solution)/shard_map/all_to_all | solution.py:142
  145.4 1.4 constant_dynamic-update-slice_fusion.31
  146.8 1.4 constant_dynamic-update-slice_fusion.30
  148.1 1.4 constant_dynamic-update-slice_fusion.29
  149.5 1.4 constant_dynamic-update-slice_fusion.28
  150.9 1.4 constant_dynamic-update-slice_fusion.27
  152.2 1.4 constant_dynamic-update-slice_fusion.26
  153.6 1.4 constant_dynamic-update-slice_fusion.25
  155.0 1.4 constant_dynamic-update-slice_fusion.24
  156.3 1.4 constant_dynamic-update-slice_fusion.23
  157.7 1.4 constant_dynamic-update-slice_fusion.22
  159.1 1.4 constant_dynamic-update-slice_fusion.21
  160.4 1.4 constant_dynamic-update-slice_fusion.20
  164.2 1.4 constant_dynamic-update-slice_fusion.15
  165.6 1.4 constant_dynamic-update-slice_fusion.14
  166.9 1.4 constant_dynamic-update-slice_fusion.13
  168.3 1.4 constant_dynamic-update-slice_fusion.12
  169.6 1.4 constant_dynamic-update-slice_fusion.11
  171.0 1.4 constant_dynamic-update-slice_fusion.10
  172.4 1.4 constant_dynamic-update-slice_fusion.9
  173.7 1.4 constant_dynamic-update-slice_fusion.8
  175.1 1.4 constant_dynamic-update-slice_fusion.7
  176.4 1.4 constant_dynamic-update-slice_fusion.6
  177.8 1.4 constant_dynamic-update-slice_fusion.5
  179.8 2.0 fusion.23
  182.0 1.4 fusion.17
  183.5 0.6 constant_dynamic-update-slice_fusion.4
  185.3 0.6 constant_dynamic-update-slice_fusion.1
  186.5 1.4 fusion.37
  187.9 2.5 fusion.41
  190.5 8.1 %reduce-scatter.3.cloned.1.call-done = bf16[16,16,512]{2,1,0:T(8,128)(2,1)} async-done(((bf16[16,16,1024]{2,1,0:T(8,128)(2,1)}), bf16[16,16,512]{2,1,0:T(8,128)(2,1)}) %reduce-scatter.3.cloned.1.call-update) | async-done | bytes 262160 | tf_op jit(solution)/shard_map/reduce_scatter | solution.py:152
  198.6 5.6 %all-to-all-start.1 = ((bf16[16,16,512]{2,1,0:T(8,128)(2,1)}), bf16[16,16,512]{2,1,0:T(8,128)(2,1)S(1)}, u32[]{:S(2)}, u32[]{:S(2)}) async-start(bf16[16,16,512]{2,1,0:T(8,128)(2,1)} %reduce-scatter.3.cloned.1.call-done), calls=%async_computation.2 | async-start | bytes 524288 | tf_op jit(solution)/shard_map/all_to_all | solution.py:155
  204.5 9.8 %all-to-all-done.1 = bf16[16,16,512]{2,1,0:T(8,128)(2,1)S(1)} async-done(((bf16[16,16,512]{2,1,0:T(8,128)(2,1)}), bf16[16,16,512]{2,1,0:T(8,128)(2,1)S(1)}, u32[]{:S(2)}, u32[]{:S(2)}) %all-to-all-start.1) | async-done | bytes 262176 | tf_op jit(solution)/shard_map/all_to_all | solution.py:155
  214.3 44.1 %reduce-scatter.5.cloned.1.call-done = f32[16,512]{1,0:T(8,128)} async-done(((f32[256,512]{1,0:T(8,128)}), f32[16,512]{1,0:T(8,128)}) %reduce-scatter.5.cloned.1.call-update) | async-done | bytes 32784 | tf_op jit(solution)/shard_map/reduce_scatter | solution.py:181
  258.4 1.1 fusion.60
  259.4 4.9 %all-reduce = (f32[16]{0:T(128)S(1)}, f32[16]{0:T(128)S(1)}) all-reduce(f32[16]{0:T(128)S(1)} %get-tuple-element.6, f32[16]{0:T(128)S(1)} %get-tuple-element.5), channel_id=1, replica_groups=mesh['ep'=16,'tp'=2] {'tp'}, use_global_device_ids=true, to_apply=%region_17.18 | all-reduce | flops 32 | bytes 256 | tf_op jit(solution)/shard_map/psum | solution.py:192
  264.4 0.7 multiply_convert_fusion.3
  (110 shorter events, 10.8 us)
Async XLA Ops:
  6.5 175.5 %copy-start = (bf16[1,704,1024]{2,1,0:T(8,128)(2,1)S(1)}, bf16[1,704,1024]{2,1,0:T(8,128)(2,1)}, u32[]{:S(2)}) copy-start(bf16[1,704,1024]{2,1,0:T(8,128)(2,1)} %param.40) | copy-start | bytes 4325380
  6.5 40.6 %all-reduce.3.cloned.1.call-start = ((), (), s32[]{:S(2)}) async-start(), calls=%async_computation.4 | async-start | bytes 131072 | tf_op jit(solution)/shard_map/psum | solution.py:132
  14.1 3.6 %copy-start.1 = (f32[16,8,64,64]{3,2,1,0:T(8,128)S(1)}, f32[16,8,64,64]{3,2,1,0:T(8,128)}, u32[]{:S(2)}) copy-start(f32[16,8,64,64]{3,2,1,0:T(8,128)} %param.25) | copy-start | bytes 6291460
  17.7 3.5 %copy-start.18 = (f32[512]{0:T(512)S(1)}, f32[512]{0:T(512)}, u32[]{:S(2)}) copy-start(f32[512]{0:T(512)} %param.36) | copy-start | bytes 6148
  17.7 29.4 %copy-start.2 = (bf16[16,1024]{1,0:T(8,128)(2,1)S(1)}, bf16[16,1024]{1,0:T(8,128)(2,1)}, u32[]{:S(2)}) copy-start(bf16[16,1024]{1,0:T(8,128)(2,1)} %param.24) | copy-start | bytes 98308
  17.7 31.4 %copy-start.17 = (f32[1024]{0:T(1024)S(1)}, f32[1024]{0:T(1024)}, u32[]{:S(2)}) copy-start(f32[1024]{0:T(1024)} %param.37) | copy-start | bytes 12292
  17.8 96.4 %copy-start.16 = (s32[16,2]{0,1:T(2,128)S(1)}, s32[16,2]{0,1:T(2,128)}, u32[]{:S(2)}) copy-start(s32[16,2]{0,1:T(2,128)} %param.46) | copy-start | bytes 388
  20.7 158.4 %copy-start.3 = (bf16[1,1024,704]{1,2,0:T(8,128)(2,1)S(1)}, bf16[1,1024,704]{1,2,0:T(8,128)(2,1)}, u32[]{:S(2)}) copy-start(bf16[1,1024,704]{1,2,0:T(8,128)(2,1)} %param.38) | copy-start | bytes 4325380
  50.1 6.1 %collective-permute-start = (bf16[16,1024]{1,0:T(8,128)(2,1)S(1)}, bf16[16,1024]{1,0:T(8,128)(2,1)S(1)}, u32[]{:S(2)}, u32[]{:S(2)}) collective-permute-start(bf16[16,1024]{1,0:T(8,128)(2,1)S(1)} %multiply_convert_fusion.2), channel_id=1, source_target_pairs={{0,2},{2,4},{4,6},{6,8},{8,10},{10,12},{12,14},{14,16},{16,18},{18... | collective-permute-start | bytes 98312 | tf_op jit(solution)/shard_map/ppermute | solution.py:170
  56.2 6.0 %collective-permute-start.1 = (bf16[16,1024]{1,0:T(8,128)(2,1)S(1)}, bf16[16,1024]{1,0:T(8,128)(2,1)S(1)}, u32[]{:S(2)}, u32[]{:S(2)}) collective-permute-start(bf16[16,1024]{1,0:T(8,128)(2,1)S(1)} %collective-permute-done), channel_id=1, source_target_pairs={{0,2},{2,4},{4,6},{6,8},{8,10},{10,12},{12,14},{14,16},{16,18},{18... | collective-permute-start | bytes 98312 | tf_op jit(solution)/shard_map/ppermute | solution.py:170
  62.2 6.0 %collective-permute-start.2 = (bf16[16,1024]{1,0:T(8,128)(2,1)S(1)}, bf16[16,1024]{1,0:T(8,128)(2,1)S(1)}, u32[]{:S(2)}, u32[]{:S(2)}) collective-permute-start(bf16[16,1024]{1,0:T(8,128)(2,1)S(1)} %collective-permute-done.1), channel_id=1, source_target_pairs={{0,2},{2,4},{4,6},{6,8},{8,10},{10,12},{12,14},{14,16},{16,18},{18... | collective-permute-start | bytes 98312 | tf_op jit(solution)/shard_map/ppermute | solution.py:170
  68.3 6.0 %collective-permute-start.3 = (bf16[16,1024]{1,0:T(8,128)(2,1)S(1)}, bf16[16,1024]{1,0:T(8,128)(2,1)S(1)}, u32[]{:S(2)}, u32[]{:S(2)}) collective-permute-start(bf16[16,1024]{1,0:T(8,128)(2,1)S(1)} %collective-permute-done.2), channel_id=1, source_target_pairs={{0,2},{2,4},{4,6},{6,8},{8,10},{10,12},{12,14},{14,16},{16,18},{18... | collective-permute-start | bytes 98312 | tf_op jit(solution)/shard_map/ppermute | solution.py:170
  74.3 0.6 copy-start.5
  74.9 6.0 %collective-permute-start.4 = (bf16[16,1024]{1,0:T(8,128)(2,1)S(1)}, bf16[16,1024]{1,0:T(8,128)(2,1)S(1)}, u32[]{:S(2)}, u32[]{:S(2)}) collective-permute-start(bf16[16,1024]{1,0:T(8,128)(2,1)S(1)} %collective-permute-done.3), channel_id=1, source_target_pairs={{0,2},{2,4},{4,6},{6,8},{8,10},{10,12},{12,14},{14,16},{16,18},{18... | collective-permute-start | bytes 98312 | tf_op jit(solution)/shard_map/ppermute | solution.py:170
  80.9 0.6 copy-start.7
  81.5 6.0 %collective-permute-start.5 = (bf16[16,1024]{1,0:T(8,128)(2,1)S(1)}, bf16[16,1024]{1,0:T(8,128)(2,1)S(1)}, u32[]{:S(2)}, u32[]{:S(2)}) collective-permute-start(bf16[16,1024]{1,0:T(8,128)(2,1)S(1)} %collective-permute-done.4), channel_id=1, source_target_pairs={{0,2},{2,4},{4,6},{6,8},{8,10},{10,12},{12,14},{14,16},{16,18},{18... | collective-permute-start | bytes 98312 | tf_op jit(solution)/shard_map/ppermute | solution.py:170
  87.6 0.6 copy-start.8
  88.2 6.0 %collective-permute-start.6 = (bf16[16,1024]{1,0:T(8,128)(2,1)S(1)}, bf16[16,1024]{1,0:T(8,128)(2,1)S(1)}, u32[]{:S(2)}, u32[]{:S(2)}) collective-permute-start(bf16[16,1024]{1,0:T(8,128)(2,1)S(1)} %collective-permute-done.5), channel_id=1, source_target_pairs={{0,2},{2,4},{4,6},{6,8},{8,10},{10,12},{12,14},{14,16},{16,18},{18... | collective-permute-start | bytes 98312 | tf_op jit(solution)/shard_map/ppermute | solution.py:170
  94.2 0.6 copy-start.9
  94.8 6.0 %collective-permute-start.7 = (bf16[16,1024]{1,0:T(8,128)(2,1)S(1)}, bf16[16,1024]{1,0:T(8,128)(2,1)S(1)}, u32[]{:S(2)}, u32[]{:S(2)}) collective-permute-start(bf16[16,1024]{1,0:T(8,128)(2,1)S(1)} %collective-permute-done.6), channel_id=1, source_target_pairs={{0,2},{2,4},{4,6},{6,8},{8,10},{10,12},{12,14},{14,16},{16,18},{18... | collective-permute-start | bytes 98312 | tf_op jit(solution)/shard_map/ppermute | solution.py:170
  100.9 0.6 copy-start.10
  101.5 6.0 %collective-permute-start.8 = (bf16[16,1024]{1,0:T(8,128)(2,1)S(1)}, bf16[16,1024]{1,0:T(8,128)(2,1)S(1)}, u32[]{:S(2)}, u32[]{:S(2)}) collective-permute-start(bf16[16,1024]{1,0:T(8,128)(2,1)S(1)} %collective-permute-done.7), channel_id=1, source_target_pairs={{0,2},{2,4},{4,6},{6,8},{8,10},{10,12},{12,14},{14,16},{16,18},{18... | collective-permute-start | bytes 98312 | tf_op jit(solution)/shard_map/ppermute | solution.py:170
  107.5 0.6 copy-start.11
  108.1 6.0 %collective-permute-start.9 = (bf16[16,1024]{1,0:T(8,128)(2,1)S(1)}, bf16[16,1024]{1,0:T(8,128)(2,1)S(1)}, u32[]{:S(2)}, u32[]{:S(2)}) collective-permute-start(bf16[16,1024]{1,0:T(8,128)(2,1)S(1)} %collective-permute-done.8), channel_id=1, source_target_pairs={{0,2},{2,4},{4,6},{6,8},{8,10},{10,12},{12,14},{14,16},{16,18},{18... | collective-permute-start | bytes 98312 | tf_op jit(solution)/shard_map/ppermute | solution.py:170
  114.1 25.4 %copy-start.12 = (bf16[16,1024]{1,0:T(8,128)(2,1)}, bf16[16,1024]{1,0:T(8,128)(2,1)S(1)}, u32[]{:S(2)}) copy-start(bf16[16,1024]{1,0:T(8,128)(2,1)S(1)} %collective-permute-done.9) | copy-start | bytes 98308
  114.1 6.0 %collective-permute-start.10 = (bf16[16,1024]{1,0:T(8,128)(2,1)S(1)}, bf16[16,1024]{1,0:T(8,128)(2,1)S(1)}, u32[]{:S(2)}, u32[]{:S(2)}) collective-permute-start(bf16[16,1024]{1,0:T(8,128)(2,1)S(1)} %collective-permute-done.9), channel_id=1, source_target_pairs={{0,2},{2,4},{4,6},{6,8},{8,10},{10,12},{12,14},{14,16},{16,18},{18... | collective-permute-start | bytes 98312 | tf_op jit(solution)/shard_map/ppermute | solution.py:170
  120.2 19.3 %copy-start.13 = (bf16[16,1024]{1,0:T(8,128)(2,1)}, bf16[16,1024]{1,0:T(8,128)(2,1)S(1)}, u32[]{:S(2)}) copy-start(bf16[16,1024]{1,0:T(8,128)(2,1)S(1)} %collective-permute-done.10) | copy-start | bytes 98308
  120.2 6.0 %collective-permute-start.11 = (bf16[16,1024]{1,0:T(8,128)(2,1)S(1)}, bf16[16,1024]{1,0:T(8,128)(2,1)S(1)}, u32[]{:S(2)}, u32[]{:S(2)}) collective-permute-start(bf16[16,1024]{1,0:T(8,128)(2,1)S(1)} %collective-permute-done.10), channel_id=1, source_target_pairs={{0,2},{2,4},{4,6},{6,8},{8,10},{10,12},{12,14},{14,16},{16,18},{18... | collective-permute-start | bytes 98312 | tf_op jit(solution)/shard_map/ppermute | solution.py:170
  126.2 13.3 %copy-start.14 = (bf16[16,1024]{1,0:T(8,128)(2,1)}, bf16[16,1024]{1,0:T(8,128)(2,1)S(1)}, u32[]{:S(2)}) copy-start(bf16[16,1024]{1,0:T(8,128)(2,1)S(1)} %collective-permute-done.11) | copy-start | bytes 98308
  126.2 6.0 %collective-permute-start.12 = (bf16[16,1024]{1,0:T(8,128)(2,1)S(1)}, bf16[16,1024]{1,0:T(8,128)(2,1)S(1)}, u32[]{:S(2)}, u32[]{:S(2)}) collective-permute-start(bf16[16,1024]{1,0:T(8,128)(2,1)S(1)} %collective-permute-done.11), channel_id=1, source_target_pairs={{0,2},{2,4},{4,6},{6,8},{8,10},{10,12},{12,14},{14,16},{16,18},{18... | collective-permute-start | bytes 98312 | tf_op jit(solution)/shard_map/ppermute | solution.py:170
  132.3 7.3 %copy-start.15 = (bf16[16,1024]{1,0:T(8,128)(2,1)}, bf16[16,1024]{1,0:T(8,128)(2,1)S(1)}, u32[]{:S(2)}) copy-start(bf16[16,1024]{1,0:T(8,128)(2,1)S(1)} %collective-permute-done.12) | copy-start | bytes 98308
  132.3 6.1 %collective-permute-start.13 = (bf16[16,1024]{1,0:T(8,128)(2,1)S(1)}, bf16[16,1024]{1,0:T(8,128)(2,1)}, u32[]{:S(2)}, u32[]{:S(2)}) collective-permute-start(bf16[16,1024]{1,0:T(8,128)(2,1)S(1)} %collective-permute-done.12), channel_id=1, source_target_pairs={{0,2},{2,4},{4,6},{6,8},{8,10},{10,12},{12,14},{14,16},{16,18},{18... | collective-permute-start | bytes 98312 | tf_op jit(solution)/shard_map/ppermute | solution.py:170
  138.4 7.0 %collective-permute-start.14 = (bf16[16,1024]{1,0:T(8,128)(2,1)}, bf16[16,1024]{1,0:T(8,128)(2,1)}, u32[]{:S(2)}, u32[]{:S(2)}) collective-permute-start(bf16[16,1024]{1,0:T(8,128)(2,1)} %collective-permute-done.13), channel_id=1, source_target_pairs={{0,2},{2,4},{4,6},{6,8},{8,10},{10,12},{12,14},{14,16},{16,18},{18... | collective-permute-start | bytes 98312 | tf_op jit(solution)/shard_map/ppermute | solution.py:170
  139.5 39.6 %all-to-all-start = ((bf16[16,16,1024]{2,1,0:T(8,128)(2,1)}), bf16[16,16,1024]{2,1,0:T(8,128)(2,1)S(1)}, u32[]{:S(2)}, u32[]{:S(2)}) async-start(bf16[16,16,1024]{2,1,0:T(8,128)(2,1)} %bitcast.8), calls=%async_computation | async-start | bytes 1048576 | tf_op jit(solution)/shard_map/all_to_all | solution.py:142
  145.4 53.3 %reduce-scatter.3.cloned.1.call-start = ((), (), s32[]{:S(2)}) async-start(), calls=%async_computation.5 | async-start | bytes 786432 | tf_op jit(solution)/shard_map/reduce_scatter | solution.py:152
  179.8 3.7 %copy-start.6 = (bf16[16,1024]{1,0:T(8,128)(2,1)S(1)}, bf16[16,1024]{1,0:T(8,128)(2,1)}, u32[]{:S(2)}) copy-start(bf16[16,1024]{1,0:T(8,128)(2,1)} %copy-done.5) | copy-start | bytes 98308
  179.8 6.8 %copy-start.4 = (bf16[176,1024]{1,0:T(8,128)(2,1)S(1)}, bf16[176,1024]{1,0:T(8,128)(2,1)}, u32[]{:S(2)}) copy-start(bf16[176,1024]{1,0:T(8,128)(2,1)} %param.42) | copy-start | bytes 1081348
  179.8 8.1 %copy-start.23 = (bf16[176,512]{1,0:T(8,128)(2,1)S(1)}, bf16[176,512]{1,0:T(8,128)(2,1)}, u32[]{:S(2)}) copy-start(bf16[176,512]{1,0:T(8,128)(2,1)} %param.43) | copy-start | bytes 540676
  181.8 6.1 %copy-start.22 = (bf16[176,1024]{1,0:T(8,128)(2,1)S(1)}, bf16[176,1024]{1,0:T(8,128)(2,1)}, u32[]{:S(2)}) copy-start(bf16[176,1024]{1,0:T(8,128)(2,1)} %param.41) | copy-start | bytes 1081348
  181.8 22.4 %copy-start.19 = (bf16[1024]{0:T(1024)(128)(2,1)S(1)}, bf16[1024]{0:T(1024)(128)(2,1)}, u32[]{:S(2)}) copy-start(bf16[1024]{0:T(1024)(128)(2,1)} %param.44) | copy-start | bytes 6148
  181.8 22.5 %copy-start.21 = (f32[16,2]{0,1:T(2,128)S(1)}, f32[16,2]{0,1:T(2,128)}, u32[]{:S(2)}) copy-start(f32[16,2]{0,1:T(2,128)} %param.47) | copy-start | bytes 388
  182.0 82.4 %copy-start.20 = (f32[512]{0:T(512)S(1)}, f32[512]{0:T(512)}, u32[]{:S(2)}) copy-start(f32[512]{0:T(512)} %param.45) | copy-start | bytes 6148
  183.4 74.9 %reduce-scatter.5.cloned.1.call-start = ((), (), s32[]{:S(2)}) async-start(), calls=%async_computation.6 | async-start | bytes 557056 | tf_op jit(solution)/shard_map/reduce_scatter | solution.py:181
  198.6 15.6 %all-to-all-start.1 = ((bf16[16,16,512]{2,1,0:T(8,128)(2,1)}), bf16[16,16,512]{2,1,0:T(8,128)(2,1)S(1)}, u32[]{:S(2)}, u32[]{:S(2)}) async-start(bf16[16,16,512]{2,1,0:T(8,128)(2,1)} %reduce-scatter.3.cloned.1.call-done), calls=%async_computation.2 | async-start | bytes 524288 | tf_op jit(solution)/shard_map/all_to_all | solution.py:155
Sparse Core Ops, SparseCore 0:
  23.4 23.6 all-reduce.2
  183.6 15.0 reduce-scatter.2
  202.2 56.1 reduce-scatter.4
